TPU v7x, 32 devices: a whole 2x2x4 slice. The times are simulated.
32 devices in a mesh: fs: 8 (over z, y), tp: 4 (over x, core).
Axes of the slice: x: 2, y: 2, z: 4, core: 2. Of those that a mesh axis runs over, the one named last changes fastest.
Arguments:
- tokens: bfloat16 [8192, 2048], P('fs'), may hold values from -6 to 6
- norm_gain: float32 [2048], P('fs'), may hold values from 0.1 to 1.9
- gate_train: float32 [8, 2048, 768], P(None, 'fs', 'tp'), may hold values from -0.125 to 0.125
- up_train: float32 [8, 2048, 768], P(None, 'fs', 'tp'), may hold values from -0.125 to 0.125
- down_train: float32 [8, 768, 2048], P(None, 'fs', 'tp'), may hold values from -0.21875 to 0.21875
- expert_ids: int32 [8192, 2], P('fs'), may hold values from 0 to 7, all different within a row; in each aligned block of 1024 rows (0 to 1023, 1024 to 2047, ...) at most 512 rows name the same one
- route_weights: float32 [8192, 2], P('fs'), may hold values from 0.1 to 1
Outputs:
- gate_serve: bfloat16 [8, 2048, 768], P('fs', None, 'tp')
- up_serve: bfloat16 [8, 2048, 768], P('fs', None, 'tp')
- down_serve: bfloat16 [8, 768, 2048], P('fs', 'tp')
- mixed: bfloat16 [8192, 2048], P('fs', 'tp')
Inputs may be any that keep to these rules, and one draw needn't show every extreme that they name: `expert_ids`: each row names 2 different experts. Within each aligned block of 1024 rows no expert is named more than 512 times, and in every block some expert is named exactly 512 times; every expert is named somewhere.
All inputs are finite; a program needn't handle non-finite values.
Results may differ from a plain program's by a relative error of at most 0.011.
Values may be sent and summed in bfloat16 or wider, within the bound.
No kernel may reach another device: no remote copies, remote signals or barrier semaphores. Data moves between devices by JAX's collectives and lax.ppermute only.
A program may use at most 128 MiB of HBM per device.

v0:
```python
import jax
import jax.numpy as jnp
from jax import lax
from jax.sharding import PartitionSpec as P

epsilon = 1e-06


def on_device(tokens, norm_gain, gate_train, up_train, down_train, expert_ids, route_weights):
    fs_count = lax.axis_size("fs")
    tp_count = lax.axis_size("tp")
    experts = gate_train.shape[0]
    local_experts = experts // fs_count
    gate_cast = (norm_gain[None, :, None] * gate_train).astype(jnp.bfloat16)
    up_cast = (norm_gain[None, :, None] * up_train).astype(jnp.bfloat16)
    gate_serve, up_serve = (
        lax.all_to_all(gate_cast, "fs", split_axis=0, concat_axis=1, tiled=True),
        lax.all_to_all(up_cast, "fs", split_axis=0, concat_axis=1, tiled=True),
    )
    down_serve = lax.all_to_all(
        lax.all_to_all(
            down_train.astype(jnp.bfloat16), "fs", split_axis=0, concat_axis=1, tiled=True
        ),
        "tp",
        split_axis=1,
        concat_axis=2,
        tiled=True,
    )
    tok_float = tokens.astype(jnp.float32)
    normed = (
        tok_float * lax.rsqrt(jnp.mean(tok_float * tok_float, axis=-1, keepdims=True) + epsilon)
    ).astype(jnp.bfloat16)
    tok_rows, picks = expert_ids.shape
    width = tokens.shape[1]
    capacity = 2 * tok_rows * picks // experts
    flat_ids = expert_ids.reshape(-1)
    onehot = (flat_ids[:, None] == jnp.arange(experts, dtype=jnp.int32)[None, :]).astype(jnp.int32)
    slot_rank = jnp.sum((jnp.cumsum(onehot, axis=0) - onehot) * onehot, axis=1)
    target = (flat_ids * capacity + slot_rank).reshape(tok_rows, picks)
    slot_ids = jnp.arange(experts * capacity, dtype=jnp.int32)
    dispatch = jnp.zeros((experts * capacity, tok_rows), jnp.bfloat16)
    for pick in range(picks):
        dispatch = dispatch + (slot_ids[:, None] == target[None, :, pick]).astype(jnp.bfloat16)
    outgoing = jnp.dot(dispatch, normed, preferred_element_type=jnp.float32).astype(jnp.bfloat16)
    outgoing = outgoing.reshape(experts, capacity, width)
    quarter = capacity // tp_count
    gate_whole, up_whole, down_whole = (
        lax.all_gather(gate_serve, "tp", axis=2, tiled=True),
        lax.all_gather(up_serve, "tp", axis=2, tiled=True),
        lax.all_gather(down_serve, "tp", axis=1, tiled=True),
    )
    share_rows = lax.dynamic_slice_in_dim(outgoing, lax.axis_index("tp") * quarter, quarter, 1)
    routed = lax.all_to_all(share_rows, "fs", split_axis=0, concat_axis=1, tiled=True)
    gate_act = jnp.einsum("erd,edf->erf", routed, gate_whole, preferred_element_type=jnp.float32)
    up_act = jnp.einsum("erd,edf->erf", routed, up_whole, preferred_element_type=jnp.float32)
    hidden = (jax.nn.silu(gate_act) * up_act).astype(jnp.bfloat16)
    row_count = hidden.shape[1]
    block_width = hidden.shape[2] // tp_count
    hidden_blocks = hidden.reshape(local_experts, row_count, tp_count, block_width)
    down_blocks = down_whole.reshape(local_experts, tp_count, block_width, width)
    partial_value = jnp.einsum(
        "erbf,ebfd->erbd", hidden_blocks, down_blocks, preferred_element_type=jnp.float32
    )
    results = jnp.sum(partial_value.astype(jnp.bfloat16).astype(jnp.float32), axis=2).astype(
        jnp.bfloat16
    )
    returned = lax.all_to_all(
        lax.all_to_all(results, "fs", split_axis=1, concat_axis=0, tiled=True),
        "tp",
        split_axis=2,
        concat_axis=1,
        tiled=True,
    )
    returned_flat = returned.reshape(experts * capacity, returned.shape[2])
    shares = route_weights / jnp.sum(route_weights, axis=-1, keepdims=True)
    mixed = jnp.zeros((tok_rows, returned_flat.shape[1]), jnp.float32)
    for pick in range(picks):
        selector = (target[:, pick][:, None] == slot_ids[None, :]).astype(jnp.bfloat16)
        picked = jnp.dot(selector, returned_flat, preferred_element_type=jnp.float32)
        mixed = mixed + shares[:, pick][:, None] * picked
    return (gate_serve, up_serve, down_serve, mixed.astype(jnp.bfloat16))


def solution(mesh):
    return jax.shard_map(
        on_device,
        mesh=mesh,
        in_specs=(
            P("fs", None),
            P("fs"),
            P(None, "fs", "tp"),
            P(None, "fs", "tp"),
            P(None, "fs", "tp"),
            P("fs", None),
            P("fs", None),
        ),
        out_specs=(P("fs", None, "tp"), P("fs", None, "tp"), P("fs", "tp", None), P("fs", "tp")),
        check_vma=False,
    )
```

profile of v0, /device:TPU:0, one launch (start us, length us, event | category | flops | bytes accessed | tf_op | source)
XLA Modules:
  0.0 500.3 jit_solution(15567781841299172667)
XLA Ops:
  7.2 0.0 copy-start.2
  7.2 0.0 copy-start.3
  7.2 3.5 multiply_convert_fusion.1
  10.7 7.3 %all-to-all-start.1 = ((bf16[8,256,192]{1,2,0:T(8,128)(2,1)}), bf16[8,256,192]{1,2,0:T(8,128)(2,1)S(1)}, u32[]{:S(2)}, u32[]{:S(2)}) async-start(bf16[8,256,192]{1,2,0:T(8,128)(2,1)} %get-tuple-element.8), calls=%async_computation.1 | async-start | bytes 1572864 | tf_op jit(solution)/shard_map/all_to_all | solution.py:18
  18.0 0.0 copy-done.2
  18.0 1.0 convert_element_type.50
  19.0 19.2 %all-to-all-done.1 = bf16[8,256,192]{1,2,0:T(8,128)(2,1)S(1)} async-done(((bf16[8,256,192]{1,2,0:T(8,128)(2,1)}), bf16[8,256,192]{1,2,0:T(8,128)(2,1)S(1)}, u32[]{:S(2)}, u32[]{:S(2)}) %all-to-all-start.1) | async-done | bytes 786464 | tf_op jit(solution)/shard_map/all_to_all | solution.py:18
  38.1 3.6 all-to-all-start.2
  41.7 0.0 copy-done.3
  41.7 0.2 copy.62
  41.9 0.3 eq.85
  42.2 0.3 eq.81
  42.5 2.3 reduce-window.6
  44.8 0.3 slice_reduce_fusion
  45.1 0.2 reduce-window.9
  45.2 16.9 %all-to-all-done.2 = bf16[8,96,512]{2,1,0:T(8,128)(2,1)S(1)} async-done(((bf16[8,96,512]{2,1,0:T(8,128)(2,1)}), bf16[8,96,512]{2,1,0:T(8,128)(2,1)S(1)}, u32[]{:S(2)}, u32[]{:S(2)}) %all-to-all-start.2) | async-done | bytes 786464 | tf_op jit(solution)/shard_map/all_to_all | solution.py:21
  62.1 3.5 all-to-all-start
  65.7 0.0 all-gather.6.cloned.1.call-start
  65.7 0.1 add_bitcast_fusion
  65.8 0.0 copy-done.1
  65.8 3.1 fusion.4
  68.9 0.4 copy.59
  69.3 1.2 all_to_all.70
  70.6 0.0 all-gather.6.cloned.1.call-update
  70.6 0.5 reduce_sum.45
  71.1 0.2 copy.64
  71.3 2.3 copy.78
  73.7 0.5 broadcast.37
  74.2 5.4 %reduce.7 = bf16[768,512]{1,0:T(8,128)(2,1)S(1)} reduce(bf16[768,1,512]{2,1,0:T(2,128)(2,1)S(1)} %bitcast.68, bf16[]{:T(256)} %broadcast.37), dimensions={1}, to_apply=%bitcast.63.reduce_sub_computation | reduce | bytes 1572866
  79.6 1.4 reshape.106
  81.0 5.0 %all-to-all-done = bf16[8,256,192]{1,2,0:T(8,128)(2,1)S(1)} async-done(((bf16[8,256,192]{1,2,0:T(8,128)(2,1)}), bf16[8,256,192]{1,2,0:T(8,128)(2,1)S(1)}, u32[]{:S(2)}, u32[]{:S(2)}) %all-to-all-start) | async-done | bytes 786464 | tf_op jit(solution)/shard_map/all_to_all | solution.py:17
  86.0 3.5 all-to-all-start.3
  89.5 11.2 %all-gather.4.cloned.1.call-start = ((), (), s32[]{:S(2)}) async-start(), calls=%async_computation.7 | async-start | bytes 3932160 | tf_op jit(solution)/shard_map/all_gather | solution.py:48
  100.8 23.5 %convolution_convert_fusion = bf16[4096,2048]{1,0:T(8,128)(2,1)} fusion(s32[1024]{0:T(1024)S(1)} %bitcast.79, s32[1024]{0:T(1024)S(1)} %bitcast.81, bf16[1024,2048]{1,0:T(8,128)(2,1)} %param.7, f32[1024]{0:T(1024)S(1)} %add_rsqrt_fusion), kind=kOutput, calls=%fused_computation.9 | convolution fusion | flops 17228103680 | bytes 20983808 | tf_op jit(solution)/shard_map/dot_general | solution.py:44
  124.3 0.4 copy.58
  124.7 1.2 all_to_all.33
  126.0 0.0 all-gather.4.cloned.1.call-update
  126.0 4.7 constant_dynamic-slice_fusion
  130.7 0.0 all-to-all-done.3
  130.7 4.6 all-to-all-start.4
  135.3 0.0 all-gather.8.cloned.1.call-start
  135.4 0.8 reshape.107
  136.2 0.2 copy.70
  136.4 1.0 copy.72
  137.3 0.0 all-gather.8.cloned.1.call-update
  137.4 0.0 all-gather.6.cloned.1.call-done
  137.4 91.7 %all-to-all-done.4 = bf16[8,128,2048]{2,1,0:T(8,128)(2,1)} async-done(((bf16[8,128,2048]{2,1,0:T(8,128)(2,1)}), bf16[8,128,2048]{2,1,0:T(8,128)(2,1)}, u32[]{:S(2)}, u32[]{:S(2)}) %all-to-all-start.4) | async-done | bytes 4194336 | tf_op jit(solution)/shard_map/all_to_all | solution.py:53
  229.1 8.3 %fusion.15 = f32[1024,768]{0,1:T(8,128)} fusion(bf16[1024,2048]{1,0:T(8,128)(2,1)} %bitcast.7, bf16[1,2048,768]{1,2,0:T(8,128)(2,1)} %all-gather.6.cloned.1.call-done), kind=kOutput, calls=%fused_computation.20 | convolution fusion | flops 3221225472 | bytes 10485760 | tf_op jit(solution)/shard_map/erd,edf->erf/dot_general | solution.py:55
  237.5 7.9 %multiply_convert_fusion = bf16[1024,768]{0,1:T(8,128)(2,1)S(1)} fusion(f32[1024,768]{0,1:T(8,128)} %fusion.15, bf16[1024,2048]{1,0:T(8,128)(2,1)} %bitcast.7, bf16[1,2048,768]{1,2,0:T(8,128)(2,1)} %all-gather.4.cloned.1.call-done), kind=kOutput, calls=%fused_computation.24 | convolution fusion | flops 3225944064 | bytes 12058624 | tf_op jit(solution)/shard_map/erd,edf->erf/dot_general | solution.py:54
  245.3 0.0 all-gather.8.cloned.1.call-done
  245.4 9.6 %convert_reduce_fusion = bf16[1024,2048]{1,0:T(8,128)(2,1)} fusion(bf16[1024,4,192]{0,2,1:T(8,128)(2,1)S(1)} %bitcast.86, bf16[4,192,2048]{2,1,0:T(8,128)(2,1)} %bitcast.85), kind=kOutput, calls=%fused_computation.1 | convolution fusion | flops 3235905536 | bytes 8912896 | tf_op jit(solution)/shard_map/erbf,ebfd->erbd/dot_general | solution.py:61
  255.0 8.6 %copy.77 = bf16[1,1024,2048]{2,0,1:T(2,128)(2,1)} copy(bf16[1,1024,2048]{2,1,0:T(8,128)(2,1)} %bitcast.70) | data formatting | bytes 8388608 | tf_op jit(solution)/shard_map/reduce_sum | solution.py:64
  263.6 26.9 %reduce.8 = bf16[1024,2048]{1,0:T(8,128)(2,1)} reduce(bf16[1024,1,2048]{2,1,0:T(2,128)(2,1)} %bitcast.65, bf16[]{:T(256)} %broadcast.37), dimensions={1}, to_apply=%bitcast.62.reduce_sub_computation | reduce | bytes 8388610
  290.5 7.8 %reshape.108 = bf16[8,2,131072]{2,1,0:T(2,128)(2,1)} reshape(bf16[1024,2048]{1,0:T(8,128)(2,1)} %reduce.8) | data formatting | bytes 8388608
  298.3 97.7 %all_to_all.90 = bf16[8,2,131072]{2,1,0:T(2,128)(2,1)} all-to-all(bf16[8,2,131072]{2,1,0:T(2,128)(2,1)} %reshape.108), channel_id=1, replica_groups=mesh['fs'=8,'tp'=4] {'fs'}, dimensions={0} | all-to-all | bytes 8388608 | tf_op jit(solution)/shard_map/all_to_all | solution.py:68
  396.0 8.7 %reshape.109 = bf16[1024,1,2048]{2,1,0:T(2,128)(2,1)} reshape(bf16[8,2,131072]{2,1,0:T(2,128)(2,1)} %all_to_all.90) | data formatting | bytes 8388608
  404.7 8.0 %copy.71 = bf16[1,1024,2048]{2,1,0:T(8,128)(2,1)} copy(bf16[1,1024,2048]{2,0,1:T(2,128)(2,1)} %bitcast.66) | data formatting | bytes 8388608
  412.7 6.8 %copy.66 = bf16[8,128,2048]{1,0,2:T(8,128)(2,1)} copy(bf16[8,128,2048]{2,1,0:T(8,128)(2,1)} %bitcast.67) | data formatting | bytes 8388608 | tf_op jit(solution)/shard_map/all_to_all | solution.py:68
  419.5 5.0 all-to-all-start.6
  424.5 0.0 copy-done.4
  424.6 48.1 %all-to-all-done.6 = bf16[8,128,2048]{1,0,2:T(8,128)(2,1)} async-done(((bf16[8,128,2048]{1,0,2:T(8,128)(2,1)}), bf16[8,128,2048]{1,0,2:T(8,128)(2,1)}, u32[]{:S(2)}, u32[]{:S(2)}) %all-to-all-start.6) | async-done | bytes 4194336 | tf_op jit(solution)/shard_map/all_to_all | solution.py:67
  472.7 7.6 %copy.68 = bf16[8,4,128,512]{3,2,1,0:T(8,128)(2,1)} copy(bf16[8,4,128,512]{2,0,3,1:T(8,128)(2,1)} %bitcast.15) | data formatting | bytes 8388608 | tf_op jit(solution)/shard_map/all_to_all | solution.py:67
  480.3 7.5 %fusion = f32[1024,512]{1,0:T(8,128)S(1)} fusion(bf16[4096,512]{1,0:T(8,128)(2,1)} %bitcast.71, s32[1024]{0:T(1024)S(1)} %bitcast.82), kind=kOutput, calls=%fused_computation.5 | convolution fusion | flops 4299161600 | bytes 6295552 | tf_op jit(solution)/shard_map/dot_general | solution.py:79
  487.8 5.6 %add_convert_fusion = bf16[1024,512]{1,0:T(8,128)(2,1)} fusion(f32[1024,512]{1,0:T(8,128)S(1)} %fusion, bf16[4096,512]{1,0:T(8,128)(2,1)S(1)} %bitcast.72, s32[1024]{0:T(1024)S(1)} %bitcast.80, f32[1024]{0:T(1024)S(1)} %bitcast.84, f32[1024]{0:T(1024)S(1)} %bitcast.83), kind=kOutput, calls=%fused_computation.25 | convolution fusion | flops 4301258752 | bytes 7352320 | tf_op jit(solution)/shard_map/dot_general | solution.py:79
  (13 shorter events, 0.1 us)
Async XLA Ops:
  7.2 10.8 %copy-start.2 = (f32[8,96,512]{2,1,0:T(8,128)S(1)}, f32[8,96,512]{2,1,0:T(8,128)}, u32[]{:S(2)}) copy-start(f32[8,96,512]{2,1,0:T(8,128)} %param.11) | copy-start | bytes 4718596
  7.2 34.5 %copy-start.3 = (s32[1024,2]{0,1:T(2,128)S(1)}, s32[1024,2]{0,1:T(2,128)}, u32[]{:S(2)}) copy-start(s32[1024,2]{0,1:T(2,128)} %param.12) | copy-start | bytes 24580
  10.7 27.5 %all-to-all-start.1 = ((bf16[8,256,192]{1,2,0:T(8,128)(2,1)}), bf16[8,256,192]{1,2,0:T(8,128)(2,1)S(1)}, u32[]{:S(2)}, u32[]{:S(2)}) async-start(bf16[8,256,192]{1,2,0:T(8,128)(2,1)} %get-tuple-element.8), calls=%async_computation.1 | async-start | bytes 1572864 | tf_op jit(solution)/shard_map/all_to_all | solution.py:18
  38.1 24.0 %all-to-all-start.2 = ((bf16[8,96,512]{2,1,0:T(8,128)(2,1)}), bf16[8,96,512]{2,1,0:T(8,128)(2,1)S(1)}, u32[]{:S(2)}, u32[]{:S(2)}) async-start(bf16[8,96,512]{2,1,0:T(8,128)(2,1)} %convert_element_type.50), calls=%async_computation.2 | async-start | bytes 1572864 | tf_op jit(solution)/shard_map/all_to_all | solution.py:21
  62.1 3.7 copy-start.1
  62.1 23.9 %all-to-all-start = ((bf16[8,256,192]{1,2,0:T(8,128)(2,1)}), bf16[8,256,192]{1,2,0:T(8,128)(2,1)S(1)}, u32[]{:S(2)}, u32[]{:S(2)}) async-start(bf16[8,256,192]{1,2,0:T(8,128)(2,1)} %get-tuple-element.9), calls=%async_computation | async-start | bytes 1572864 | tf_op jit(solution)/shard_map/all_to_all | solution.py:17
  65.7 71.7 %all-gather.6.cloned.1.call-start = ((), (), s32[]{:S(2)}) async-start(), calls=%async_computation.8 | async-start | bytes 3932160 | tf_op jit(solution)/shard_map/all_gather | solution.py:49
  86.0 44.7 %all-to-all-start.3 = ((bf16[4,2,49152]{2,1,0:T(2,128)(2,1)}), bf16[4,2,49152]{2,1,0:T(2,128)(2,1)S(1)}, u32[]{:S(2)}, u32[]{:S(2)}) async-start(bf16[4,2,49152]{2,1,0:T(2,128)(2,1)} %reshape.106), calls=%async_computation.3 | async-start | bytes 1572864 | tf_op jit(solution)/shard_map/all_to_all | solution.py:20
  89.5 147.9 %all-gather.4.cloned.1.call-start = ((), (), s32[]{:S(2)}) async-start(), calls=%async_computation.7 | async-start | bytes 3932160 | tf_op jit(solution)/shard_map/all_gather | solution.py:48
  130.7 98.4 %all-to-all-start.4 = ((bf16[8,128,2048]{2,1,0:T(8,128)(2,1)}), bf16[8,128,2048]{2,1,0:T(8,128)(2,1)}, u32[]{:S(2)}, u32[]{:S(2)}) async-start(bf16[8,128,2048]{2,1,0:T(8,128)(2,1)} %constant_dynamic-slice_fusion), calls=%async_computation.4 | async-start | bytes 8388608 | tf_op jit(solution)/shard_map/all_to_all | solution.py:53
  135.3 110.0 %all-gather.8.cloned.1.call-start = ((), (), s32[]{:S(2)}) async-start(), calls=%async_computation.9 | async-start | bytes 3932160 | tf_op jit(solution)/shard_map/all_gather | solution.py:50
  419.5 5.0 copy-start.4
  419.5 53.2 %all-to-all-start.6 = ((bf16[8,128,2048]{1,0,2:T(8,128)(2,1)}), bf16[8,128,2048]{1,0,2:T(8,128)(2,1)}, u32[]{:S(2)}, u32[]{:S(2)}) async-start(bf16[8,128,2048]{1,0,2:T(8,128)(2,1)} %copy.66), calls=%async_computation.6 | async-start | bytes 8388608 | tf_op jit(solution)/shard_map/all_to_all | solution.py:67
  480.3 7.5 %copy-start = (bf16[8,4,128,512]{3,2,1,0:T(8,128)(2,1)S(1)}, bf16[8,4,128,512]{3,2,1,0:T(8,128)(2,1)}, u32[]{:S(2)}) copy-start(bf16[8,4,128,512]{3,2,1,0:T(8,128)(2,1)} %copy.68) | copy-start | bytes 12582916
Sparse Core Ops, SparseCore 0:
  70.7 36.2 all-gather.5
  126.1 27.6 all-gather.3
  156.0 28.4 all-gather.7
where the time goes:
time: 509 us; the launch traced here: 500 us
  waiting for transfers between devices  181 us (36%)
  blocking collectives  97.7 us (19%)
  local copies, waits for them, and re-layouts  63.5 us (12%)
  matrix products  62.4 us (12%)
  other arithmetic  42.5 us (8%)
  starting transfers between devices  38.8 us (8%)
  between operations  14.4 us (3%)
    all_to_all x1, blocking collectives, on_device(): lax.all_to_all(results, 'fs', split_axis=1, concat_axis=0, tiled=True)  97.7 us
    all_to_all x1, waiting for transfers between devices, on_device(): lax.all_to_all(share_rows, 'fs', split_axis=0, concat_axis=1, tiled=True)  91.7 us
    all_to_all x1, waiting for transfers between devices, on_device(): lax.all_to_all(lax.all_to_all(results, 'fs', split_axis=1, concat_axis=0,...  48.1 us
    unnamed x3, other arithmetic  32.4 us
    unnamed x18, local copies, waits for them, and re-layouts  27.6 us
    dot_general x1, matrix products, on_device(): jnp.dot(dispatch, normed, preferred_element_type=jnp.float32)  23.5 us
    all_to_all x1, waiting for transfers between devices, on_device(): lax.all_to_all(up_cast, 'fs', split_axis=0, concat_axis=1, tiled=True)  19.2 us
    all_to_all x1, waiting for transfers between devices, on_device(): lax.all_to_all(down_train.astype(jnp.bfloat16), 'fs', split_axis=0, conca...  16.9 us
  transfers between devices with their start and end apart: 9, of which 5 were waited for; matrix products, arithmetic and copies ran while one was open for 13% of the time, Pallas kernels for 0%

commit v1 on v0

v1 whole, which is shorter than its diff:
```python
import jax
import jax.numpy as jnp
from jax import lax
from jax.experimental import pallas as pl
from jax.experimental.pallas import tpu as pltpu
from jax.sharding import PartitionSpec as P

epsilon = 1e-06


def hidden_kernel(rows_ref, gate_ref, up_ref, hidden_ref):
    rows = rows_ref[...]
    across = (((1,), (1,)), ((), ()))
    gate_act = lax.dot_general(rows, gate_ref[...], across, preferred_element_type=jnp.float32)
    up_act = lax.dot_general(rows, up_ref[...], across, preferred_element_type=jnp.float32)
    hidden_ref[...] = (gate_act / (1.0 + jnp.exp(-gate_act)) * up_act).astype(jnp.bfloat16)


def down_kernel(hidden_ref, down_ref, out_ref):
    hidden = hidden_ref[...]
    sources, shares, rows, width = out_ref.shape
    for share in range(shares):
        value = jnp.dot(hidden, down_ref[share], preferred_element_type=jnp.float32)
        out_ref[:, share] = value.astype(jnp.bfloat16).reshape(sources, rows, width)


def expert_hidden(rows, gate_t, up_t, step):
    count, width = rows.shape
    units = gate_t.shape[0]
    return pl.pallas_call(
        hidden_kernel,
        grid=(count // step,),
        in_specs=[
            pl.BlockSpec((step, width), lambda i: (i, 0)),
            pl.BlockSpec((units, width), lambda i: (0, 0)),
            pl.BlockSpec((units, width), lambda i: (0, 0)),
        ],
        out_specs=pl.BlockSpec((step, units), lambda i: (i, 0)),
        out_shape=jax.ShapeDtypeStruct((count, units), jnp.bfloat16),
        cost_estimate=pl.CostEstimate(
            flops=4 * count * units * width,
            transcendentals=count * units,
            bytes_accessed=2 * (count * width + 2 * units * width + count * units),
        ),
        name="expert_hidden",
    )(rows, gate_t, up_t)


def expert_out(hidden, down, sources, step_sources):
    count, units = hidden.shape
    shares, _, width = down.shape
    rows = count // sources
    return pl.pallas_call(
        down_kernel,
        grid=(sources // step_sources,),
        in_specs=[
            pl.BlockSpec((step_sources * rows, units), lambda i: (i, 0)),
            pl.BlockSpec((shares, units, width), lambda i: (0, 0, 0)),
        ],
        out_specs=pl.BlockSpec((step_sources, shares, rows, width), lambda i: (i, 0, 0, 0)),
        out_shape=jax.ShapeDtypeStruct((sources, shares, rows, width), jnp.bfloat16),
        cost_estimate=pl.CostEstimate(
            flops=2 * count * units * width * shares,
            transcendentals=0,
            bytes_accessed=2 * (count * units + shares * units * width + count * width * shares),
        ),
        name="expert_out",
    )(hidden, down)


def on_device(tokens, norm_gain, gate_train, up_train, down_train, expert_ids, route_weights):
    fs_count = lax.axis_size("fs")
    tp_count = lax.axis_size("tp")
    tp_index = lax.axis_index("tp")
    experts, own_rows, own_units = gate_train.shape
    assert experts == fs_count
    down_rows, down_width = down_train.shape[1:]
    tok_rows, picks = expert_ids.shape
    width = tokens.shape[1]
    capacity = 2 * tok_rows * picks // experts
    quarter = capacity // tp_count

    gain = norm_gain[None, None, :]
    gate_cast = (gain * jnp.swapaxes(gate_train, 1, 2)).astype(jnp.bfloat16)
    up_cast = (gain * jnp.swapaxes(up_train, 1, 2)).astype(jnp.bfloat16)
    down_cast = down_train.astype(jnp.bfloat16)
    cuts = down_width // own_rows
    down_cut = jnp.concatenate(
        [down_cast[:, :, cut * own_rows : (cut + 1) * own_rows] for cut in range(cuts)], axis=1
    )
    packed = jnp.concatenate([gate_cast, up_cast, down_cut], axis=1)
    arrived = lax.all_to_all(packed, "fs", split_axis=0, concat_axis=0, tiled=True)

    tok_float = tokens.astype(jnp.float32)
    normed = (
        tok_float * lax.rsqrt(jnp.mean(tok_float * tok_float, axis=-1, keepdims=True) + epsilon)
    ).astype(jnp.bfloat16)
    flat_ids = expert_ids.reshape(-1)
    onehot = (flat_ids[:, None] == jnp.arange(experts, dtype=jnp.int32)[None, :]).astype(jnp.int32)
    slot_rank = jnp.sum((jnp.cumsum(onehot, axis=0) - onehot) * onehot, axis=1)
    target = (flat_ids * capacity + slot_rank).reshape(tok_rows, picks)
    own_slots = (
        jnp.arange(experts, dtype=jnp.int32)[:, None] * capacity
        + tp_index * quarter
        + jnp.arange(quarter, dtype=jnp.int32)[None, :]
    ).reshape(-1)
    named = own_slots[:, None] == target[None, :, 0]
    for pick in range(1, picks):
        named = named | (own_slots[:, None] == target[None, :, pick])
    outgoing = jnp.dot(
        named.astype(jnp.bfloat16), normed, preferred_element_type=jnp.float32
    ).astype(jnp.bfloat16)
    outgoing = outgoing.reshape(experts, quarter, width)
    outgoing, arrived = lax.optimization_barrier((outgoing, arrived))
    routed = lax.all_to_all(outgoing, "fs", split_axis=0, concat_axis=0, tiled=True)

    def joined(part):
        return jnp.swapaxes(part, 0, 1).reshape(part.shape[1], fs_count * own_rows)

    gate_t = joined(arrived[:, :own_units])
    up_t = joined(arrived[:, own_units : 2 * own_units])
    down_own = jnp.concatenate(
        [
            arrived[
                :, 2 * own_units + cut * down_rows : 2 * own_units + (cut + 1) * down_rows
            ].reshape(fs_count * down_rows, own_rows)
            for cut in range(cuts)
        ],
        axis=1,
    )
    gate_whole = lax.all_gather(gate_t, "tp", axis=0, tiled=True)
    up_whole = lax.all_gather(up_t, "tp", axis=0, tiled=True)
    down_whole = lax.all_gather(down_own, "tp", axis=0, tiled=False)
    gate_serve = jnp.swapaxes(gate_t, 0, 1)[None]
    up_serve = jnp.swapaxes(up_t, 0, 1)[None]
    units_share = down_own.shape[0] // tp_count
    down_serve = lax.dynamic_slice_in_dim(down_whole, tp_index * units_share, units_share, 1)
    down_serve = jnp.swapaxes(down_serve, 0, 1).reshape(1, units_share, width)

    step_sources = max(1, 256 // quarter)
    hidden = expert_hidden(
        routed.reshape(fs_count * quarter, width), gate_whole, up_whole, step_sources * quarter
    )
    results = expert_out(hidden, down_whole, fs_count, step_sources)
    returned = lax.all_to_all(
        results.reshape(fs_count * tp_count, quarter, down_width),
        ("fs", "tp"),
        split_axis=0,
        concat_axis=0,
        tiled=True,
    ).reshape(experts * capacity, down_width)

    shares = route_weights / jnp.sum(route_weights, axis=-1, keepdims=True)
    slot_ids = jnp.arange(experts * capacity, dtype=jnp.int32)
    mixing = jnp.zeros((tok_rows, experts * capacity), jnp.float32)
    for pick in range(picks):
        mixing = jnp.where(
            target[:, pick][:, None] == slot_ids[None, :], shares[:, pick][:, None], mixing
        )
    mixed = jnp.dot(
        mixing.astype(jnp.bfloat16), returned, preferred_element_type=jnp.float32
    )
    return (gate_serve, up_serve, down_serve, mixed.astype(jnp.bfloat16))


def solution(mesh):
    return jax.shard_map(
        on_device,
        mesh=mesh,
        in_specs=(
            P("fs", None),
            P("fs"),
            P(None, "fs", "tp"),
            P(None, "fs", "tp"),
            P(None, "fs", "tp"),
            P("fs", None),
            P("fs", None),
        ),
        out_specs=(P("fs", None, "tp"), P("fs", None, "tp"), P("fs", "tp", None), P("fs", "tp")),
        check_vma=False,
    )
```

time: 509 us -> 304 us (0.60); the launches traced: 500 us -> 303 us
  blocking collectives: 97.7 us -> 0 us
  local copies, waits for them, and re-layouts: 63.5 us -> 7.86 us
  matrix products: 62.4 us -> 14.5 us
  waiting for transfers between devices: 181 us -> 221 us
  other arithmetic: 42.5 us -> 11.2 us
  starting transfers between devices: 38.8 us -> 15.9 us
  Pallas kernels: 0 us -> 18.6 us
    all_to_all x1 -> x0, blocking collectives: 97.7 us -> none  [on_device(): lax.all_to_all(results, 'fs', split_axis=1, concat_axis=0, tiled=True)]
    all_gather x3, waiting for transfers between devices: 0.04 us -> 51.7 us  [the longest x1 30.7 us: on_device(): up_whole = lax.all_gather(up_t, 'tp', axis=0, tiled=True)]
    dot_general x6 -> x2, matrix products: 62.4 us -> 14.5 us  [the longest x1 8.06 us: on_device(): jnp.dot(mixing.astype(jnp.bfloat16), returned, preferred_element_type=jnp...]
    unnamed x3 -> x1, other arithmetic: 32.4 us -> 0.09 us
    unnamed x18 -> x12, local copies, waits for them, and re-layouts: 27.6 us -> 1.04 us
    all_to_all x8 -> x0, local copies, waits for them, and re-layouts: 21.1 us -> none  [the longest x1 7.59 us: on_device(): lax.all_to_all(lax.all_to_all(results, 'fs', split_axis=1, concat_axis=0,...]
    pallas_call x0 -> x2, Pallas kernels: none -> 18.6 us  [the longest x1 11.3 us: expert_hidden(): pl.pallas_call(hidden_kernel, grid=(count // step,), in_specs=[pl.BlockSp...]
    all_to_all x6 -> x3, starting transfers between devices: 27.5 us -> 15.8 us  [the longest x1 7.31 us: on_device(): lax.all_to_all(packed, 'fs', split_axis=0, concat_axis=0, tiled=True)]
  transfers between devices with their start and end apart: 9 -> 6, of which waited for: 5 -> 5; matrix products, arithmetic and copies ran while one was open for 13% -> 6% of each run, Pallas kernels for 0% -> 4%
where the time goes in v1:
time: 304 us; the launch traced here: 303 us
  waiting for transfers between devices  221 us (73%)
  Pallas kernels  18.6 us (6%)
  starting transfers between devices  15.9 us (5%)
  matrix products  14.5 us (5%)
  between operations  14 us (5%)
  other arithmetic  11.2 us (4%)
  local copies, waits for them, and re-layouts  7.86 us (3%)
    all_to_all x1, waiting for transfers between devices, on_device(): lax.all_to_all(results.reshape(fs_count * tp_count, quarter, down_width),...  90.3 us
    all_to_all x1, waiting for transfers between devices, on_device(): lax.all_to_all(outgoing, 'fs', split_axis=0, concat_axis=0, tiled=True)  39.8 us
    all_to_all x1, waiting for transfers between devices, on_device(): lax.all_to_all(packed, 'fs', split_axis=0, concat_axis=0, tiled=True)  39.5 us
    all_gather x1, waiting for transfers between devices, on_device(): up_whole = lax.all_gather(up_t, 'tp', axis=0, tiled=True)  30.7 us
    all_gather x1, waiting for transfers between devices, on_device(): gate_whole = lax.all_gather(gate_t, 'tp', axis=0, tiled=True)  21 us
    pallas_call x1, Pallas kernels, expert_hidden(): pl.pallas_call(hidden_kernel, grid=(count // step,), in_specs=[pl.BlockSp...  11.3 us
    dot_general x1, matrix products, on_device(): jnp.dot(mixing.astype(jnp.bfloat16), returned, preferred_element_type=jnp...  8.06 us
    all_to_all x1, starting transfers between devices, on_device(): lax.all_to_all(packed, 'fs', split_axis=0, concat_axis=0, tiled=True)  7.31 us
  transfers between devices with their start and end apart: 6, of which 5 were waited for; matrix products, arithmetic and copies ran while one was open for 6% of the time, Pallas kernels for 4%

profile of v1, /device:TPU:0, one launch (start us, length us, event | category | flops | bytes accessed | tf_op | source)
XLA Modules:
  0.0 303.5 jit_solution(16101363336460763981)
XLA Ops:
  7.2 0.0 copy-start.1
  7.2 0.0 copy-start.2
  7.2 1.7 convert_element_type.47
  8.8 0.1 fusion.31
  8.9 0.1 copy-done.1
  9.0 0.5 copy-done.2
  9.5 1.0 fusion.23
  10.6 0.0 copy-start.3
  10.6 1.6 pad_maximum_fusion
  12.2 7.3 %all-to-all-start = ((bf16[8,576,256]{2,1,0:T(8,128)(2,1)}), bf16[8,576,256]{2,1,0:T(8,128)(2,1)S(1)}, u32[]{:S(2)}, u32[]{:S(2)}) async-start(bf16[8,576,256]{2,1,0:T(8,128)(2,1)} %pad_maximum_fusion), calls=%async_computation | async-start | bytes 4718592 | tf_op jit(solution)/shard_map/all_to_all | solution.py:92
  19.5 0.0 all-gather.5.cloned.1.call-start
  19.5 0.0 copy-done.3
  19.5 0.2 copy.27
  19.7 0.3 eq.84
  20.0 0.3 eq.80
  20.3 2.3 reduce-window.6
  22.6 0.3 slice_reduce_fusion
  22.9 0.2 reduce-window.9
  23.0 0.1 add_bitcast_fusion
  23.2 0.5 reduce_sum.30
  23.7 0.2 copy.29
  23.9 0.0 copy-start
  23.9 0.1 add_bitcast_fusion.1
  23.9 3.2 %fusion = f32[1024]{0:T(1024)S(1)} fusion(bf16[1024,2048]{1,0:T(8,128)(2,1)} %param.7), kind=kLoop, calls=%fused_computation.5 | loop fusion | flops 6290432 | bytes 4198400 | tf_op jit(solution)/shard_map/reduce_sum | solution.py:96
  27.2 0.1 copy-done
  27.3 6.5 %fusion.14 = bf16[1024,2048]{1,0:T(8,128)(2,1)} fusion(bf16[1024,2048]{1,0:T(8,128)(2,1)S(1)} %copy-done, f32[1024]{0:T(1024)S(1)} %add_rsqrt_fusion, s32[1024]{0:T(1024)S(1)} %bitcast.68, s32[1024]{0:T(1024)S(1)} %bitcast.66, s32[1024]{0:T(1024)S(1)} %add_bitcast_fusion.1), kind=kOutput, calls=%fused_computation.18 | convolution fusion | flops 4306501632 | bytes 8404992 | tf_op jit(solution)/shard_map/dot_general | solution.py:110
  33.8 39.5 %all-to-all-done = bf16[8,576,256]{2,1,0:T(8,128)(2,1)S(1)} async-done(((bf16[8,576,256]{2,1,0:T(8,128)(2,1)}), bf16[8,576,256]{2,1,0:T(8,128)(2,1)S(1)}, u32[]{:S(2)}, u32[]{:S(2)}) %all-to-all-start) | async-done | bytes 2359328 | tf_op jit(solution)/shard_map/all_to_all | solution.py:92
  73.3 0.1 slice_bitcast_fusion
  73.4 1.0 copy.33
  74.4 0.0 all-gather.5.cloned.1.call-update
  74.4 0.0 all-gather.7.cloned.1.call-start
  74.5 1.0 copy.34
  75.5 0.0 all-gather.7.cloned.1.call-update
  75.5 4.6 %all-to-all-start.1 = ((bf16[8,128,2048]{2,1,0:T(8,128)(2,1)}), bf16[8,128,2048]{2,1,0:T(8,128)(2,1)}, u32[]{:S(2)}, u32[]{:S(2)}) async-start(bf16[8,128,2048]{2,1,0:T(8,128)(2,1)} %bitcast.55), calls=%async_computation.1 | async-start | bytes 8388608 | tf_op jit(solution)/shard_map/all_to_all | solution.py:115
  80.1 0.0 all-gather.9.cloned.1.call-start
  80.1 0.1 fusion.30
  80.2 0.9 pad_maximum_fusion.1
  81.1 0.0 all-gather.9.cloned.1.call-update
  81.1 21.0 %all-gather.5.cloned.1.call-done.gate_ref = bf16[768,2048]{1,0:T(8,128)(2,1)} async-done(((bf16[192,2048]{1,0:T(8,128)(2,1)}), bf16[768,2048]{1,0:T(8,128)(2,1)}) %all-gather.5.cloned.1.call-update) | async-done | bytes 3145744 | tf_op jit(solution)/shard_map/all_gather | solution.py:131
  102.1 30.7 %all-gather.7.cloned.1.call-done.up_ref = bf16[768,2048]{1,0:T(8,128)(2,1)} async-done(((bf16[192,2048]{1,0:T(8,128)(2,1)}), bf16[768,2048]{1,0:T(8,128)(2,1)}) %all-gather.7.cloned.1.call-update) | async-done | bytes 3145744 | tf_op jit(solution)/shard_map/all_gather | solution.py:132
  132.8 39.8 %all-to-all-done.1 = bf16[8,128,2048]{2,1,0:T(8,128)(2,1)} async-done(((bf16[8,128,2048]{2,1,0:T(8,128)(2,1)}), bf16[8,128,2048]{2,1,0:T(8,128)(2,1)}, u32[]{:S(2)}, u32[]{:S(2)}) %all-to-all-start.1) | async-done | bytes 4194336 | tf_op jit(solution)/shard_map/all_to_all | solution.py:115
  172.6 11.3 %expert_hidden.1.hidden_ref = bf16[1024,768]{1,0:T(8,128)(2,1)} custom-call(bf16[1024,2048]{1,0:T(8,128)(2,1)} %bitcast.19.rows_ref, bf16[768,2048]{1,0:T(8,128)(2,1)} %all-gather.5.cloned.1.call-done.gate_ref, bf16[768,2048]{1,0:T(8,128)(2,1)} %all-gather.7.cloned.1.call-done.up_ref), custom_call_target="tpu_custom_call" | custom-call | flops 6442450944 | bytes 12058624 | tf_op jit(solution)/shard_map/expert_hidden/pallas_call | solution.py:30
  184.0 0.0 all-gather.9.cloned.1.call-done
  184.0 7.3 %expert_out.1 = bf16[8,4,128,512]{3,2,1,0:T(8,128)(2,1)} custom-call(bf16[1024,768]{1,0:T(8,128)(2,1)} %expert_hidden.1.hidden_ref, bf16[4,768,512]{2,1,0:T(8,128)(2,1)} %bitcast.63), custom_call_target="tpu_custom_call" | custom-call | flops 3221225472 | bytes 8912896 | tf_op jit(solution)/shard_map/expert_out/pallas_call | solution.py:53
  191.2 0.0 copy-start.4
  191.2 4.0 %all-to-all-start.2 = ((bf16[32,128,512]{2,1,0:T(8,128)(2,1)}), bf16[32,128,512]{2,1,0:T(8,128)(2,1)}, u32[]{:S(2)}, u32[]{:S(2)}) async-start(bf16[32,128,512]{2,1,0:T(8,128)(2,1)} %bitcast.56), calls=%async_computation.2 | async-start | bytes 8388608 | tf_op jit(solution)/shard_map/all_to_all | solution.py:145
  195.2 0.0 copy-done.4
  195.3 1.2 dynamic-slice_bitcast_fusion
  196.5 0.6 copy.32
  197.1 1.5 reshape.94
  198.6 90.3 %all-to-all-done.2 = bf16[32,128,512]{2,1,0:T(8,128)(2,1)} async-done(((bf16[32,128,512]{2,1,0:T(8,128)(2,1)}), bf16[32,128,512]{2,1,0:T(8,128)(2,1)}, u32[]{:S(2)}, u32[]{:S(2)}) %all-to-all-start.2) | async-done | bytes 4194336 | tf_op jit(solution)/shard_map/all_to_all | solution.py:145
  288.9 8.1 %fusion.22 = bf16[1024,512]{1,0:T(8,128)(2,1)} fusion(bf16[4096,512]{1,0:T(8,128)(2,1)} %bitcast.21, f32[1024]{0:T(1024)S(1)} %bitcast.71, s32[1024]{0:T(1024)S(1)} %bitcast.67, f32[1024]{0:T(1024)S(1)} %bitcast.70, s32[1024]{0:T(1024)S(1)} %bitcast.69), kind=kOutput, calls=%fused_computation.25 | convolution fusion | flops 4312268800 | bytes 5259264 | tf_op jit(solution)/shard_map/dot_general | solution.py:160
  (9 shorter events, 0.1 us)
Async XLA Ops:
  7.2 1.9 copy-start.1
  7.2 2.3 copy-start.2
  10.6 8.9 %copy-start.3 = (s32[1024,2]{0,1:T(2,128)S(1)}, s32[1024,2]{0,1:T(2,128)}, u32[]{:S(2)}) copy-start(s32[1024,2]{0,1:T(2,128)} %param.12) | copy-start | bytes 24580
  12.2 61.2 %all-to-all-start = ((bf16[8,576,256]{2,1,0:T(8,128)(2,1)}), bf16[8,576,256]{2,1,0:T(8,128)(2,1)S(1)}, u32[]{:S(2)}, u32[]{:S(2)}) async-start(bf16[8,576,256]{2,1,0:T(8,128)(2,1)} %pad_maximum_fusion), calls=%async_computation | async-start | bytes 4718592 | tf_op jit(solution)/shard_map/all_to_all | solution.py:92
  19.5 82.7 %all-gather.5.cloned.1.call-start = ((), (), s32[]{:S(2)}) async-start(), calls=%async_computation.3 | async-start | bytes 3932160 | tf_op jit(solution)/shard_map/all_gather | solution.py:131
  23.9 3.5 %copy-start = (bf16[1024,2048]{1,0:T(8,128)(2,1)S(1)}, bf16[1024,2048]{1,0:T(8,128)(2,1)}, u32[]{:S(2)}) copy-start(bf16[1024,2048]{1,0:T(8,128)(2,1)} %param.7) | copy-start | bytes 12582916
  74.4 58.4 %all-gather.7.cloned.1.call-start = ((), (), s32[]{:S(2)}) async-start(), calls=%async_computation.4 | async-start | bytes 3932160 | tf_op jit(solution)/shard_map/all_gather | solution.py:132
  75.5 97.1 %all-to-all-start.1 = ((bf16[8,128,2048]{2,1,0:T(8,128)(2,1)}), bf16[8,128,2048]{2,1,0:T(8,128)(2,1)}, u32[]{:S(2)}, u32[]{:S(2)}) async-start(bf16[8,128,2048]{2,1,0:T(8,128)(2,1)} %bitcast.55), calls=%async_computation.1 | async-start | bytes 8388608 | tf_op jit(solution)/shard_map/all_to_all | solution.py:115
  80.1 103.9 %all-gather.9.cloned.1.call-start = ((), (), s32[]{:S(2)}) async-start(), calls=%async_computation.5 | async-start | bytes 3932160 | tf_op jit(solution)/shard_map/all_gather | solution.py:133
  191.2 4.0 %copy-start.4 = (f32[1024,2]{0,1:T(2,128)S(1)}, f32[1024,2]{0,1:T(2,128)}, u32[]{:S(2)}) copy-start(f32[1024,2]{0,1:T(2,128)} %param.13) | copy-start | bytes 24580
  191.2 97.7 %all-to-all-start.2 = ((bf16[32,128,512]{2,1,0:T(8,128)(2,1)}), bf16[32,128,512]{2,1,0:T(8,128)(2,1)}, u32[]{:S(2)}, u32[]{:S(2)}) async-start(bf16[32,128,512]{2,1,0:T(8,128)(2,1)} %bitcast.56), calls=%async_computation.2 | async-start | bytes 8388608 | tf_op jit(solution)/shard_map/all_to_all | solution.py:145
Sparse Core Ops, SparseCore 0:
  74.6 27.5 all-gather.4
  104.3 28.4 all-gather.6
  135.0 28.4 all-gather.8

commit v2 on v1

--- a/solution.py
+++ b/solution.py
@@ -8,7 +8,7 @@
 epsilon = 1e-06
 
 
-def hidden_kernel(rows_ref, gate_ref, up_ref, hidden_ref):
+def hidden_kernel(first_ref, rows_ref, gate_ref, up_ref, hidden_ref):
     rows = rows_ref[...]
     across = (((1,), (1,)), ((), ()))
     gate_act = lax.dot_general(rows, gate_ref[...], across, preferred_element_type=jnp.float32)
@@ -24,18 +24,22 @@
         out_ref[:, share] = value.astype(jnp.bfloat16).reshape(sources, rows, width)
 
 
-def expert_hidden(rows, gate_t, up_t, step):
-    count, width = rows.shape
+def expert_hidden(first, rows, gate_t, up_t, step):
+    width = rows.shape[1]
+    count = rows.shape[0] // 2
     units = gate_t.shape[0]
     return pl.pallas_call(
         hidden_kernel,
-        grid=(count // step,),
-        in_specs=[
-            pl.BlockSpec((step, width), lambda i: (i, 0)),
-            pl.BlockSpec((units, width), lambda i: (0, 0)),
-            pl.BlockSpec((units, width), lambda i: (0, 0)),
-        ],
-        out_specs=pl.BlockSpec((step, units), lambda i: (i, 0)),
+        grid_spec=pltpu.PrefetchScalarGridSpec(
+            num_scalar_prefetch=1,
+            grid=(count // step,),
+            in_specs=[
+                pl.BlockSpec((step, width), lambda i, first_ref: (first_ref[0] + i, 0)),
+                pl.BlockSpec((units, width), lambda i, first_ref: (0, 0)),
+                pl.BlockSpec((units, width), lambda i, first_ref: (0, 0)),
+            ],
+            out_specs=pl.BlockSpec((step, units), lambda i, first_ref: (i, 0)),
+        ),
         out_shape=jax.ShapeDtypeStruct((count, units), jnp.bfloat16),
         cost_estimate=pl.CostEstimate(
             flops=4 * count * units * width,
@@ -43,7 +47,7 @@
             bytes_accessed=2 * (count * width + 2 * units * width + count * units),
         ),
         name="expert_hidden",
-    )(rows, gate_t, up_t)
+    )(first, rows, gate_t, up_t)
 
 
 def expert_out(hidden, down, sources, step_sources):
@@ -137,29 +141,56 @@
     down_serve = lax.dynamic_slice_in_dim(down_whole, tp_index * units_share, units_share, 1)
     down_serve = jnp.swapaxes(down_serve, 0, 1).reshape(1, units_share, width)
 
-    step_sources = max(1, 256 // quarter)
-    hidden = expert_hidden(
-        routed.reshape(fs_count * quarter, width), gate_whole, up_whole, step_sources * quarter
-    )
-    results = expert_out(hidden, down_whole, fs_count, step_sources)
-    returned = lax.all_to_all(
-        results.reshape(fs_count * tp_count, quarter, down_width),
-        ("fs", "tp"),
-        split_axis=0,
-        concat_axis=0,
-        tiled=True,
-    ).reshape(experts * capacity, down_width)
+    half = fs_count // 2
+    assert 2 * half == fs_count
+    own_half = lax.axis_index("fs") // half
+    mirror = [(source, (source + half) % fs_count) for source in range(fs_count)]
+    members = half * tp_count
+    halves = [list(range(members)), list(range(members, 2 * members))]
+    half_slots = half * capacity
+    step_sources = min(half, max(1, 256 // quarter))
+    rows = routed.reshape(fs_count * quarter, width)
+    blocks = half // step_sources
+
+    def apply_half(which, rows):
+        first = (which * blocks).astype(jnp.int32).reshape(1)
+        hidden = expert_hidden(first, rows, gate_whole, up_whole, step_sources * quarter)
+        return expert_out(hidden, down_whole, half, step_sources)
+
+    def spread(results):
+        return lax.all_to_all(
+            results.reshape(members, quarter, down_width),
+            ("fs", "tp"),
+            split_axis=0,
+            concat_axis=0,
+            axis_index_groups=halves,
+            tiled=True,
+        ).reshape(half_slots, down_width)
+
+    slot_ids = own_half * half_slots + jnp.arange(half_slots, dtype=jnp.int32)
+
+    def mix(target, shares, values):
+        mixing = jnp.zeros((tok_rows, half_slots), jnp.float32)
+        for pick in range(picks):
+            mixing = jnp.where(
+                target[:, pick][:, None] == slot_ids[None, :], shares[:, pick][:, None], mixing
+            )
+        return jnp.dot(mixing.astype(jnp.bfloat16), values, preferred_element_type=jnp.float32)
 
     shares = route_weights / jnp.sum(route_weights, axis=-1, keepdims=True)
-    slot_ids = jnp.arange(experts * capacity, dtype=jnp.int32)
-    mixing = jnp.zeros((tok_rows, experts * capacity), jnp.float32)
-    for pick in range(picks):
-        mixing = jnp.where(
-            target[:, pick][:, None] == slot_ids[None, :], shares[:, pick][:, None], mixing
-        )
-    mixed = jnp.dot(
-        mixing.astype(jnp.bfloat16), returned, preferred_element_type=jnp.float32
-    )
+    mirror_target = lax.ppermute(target, "fs", mirror)
+    mirror_shares = lax.ppermute(shares, "fs", mirror)
+    far_results = apply_half(1 - own_half, rows)
+    far_results, rows, mirror_target, mirror_shares = lax.optimization_barrier(
+        (far_results, rows, mirror_target, mirror_shares)
+    )
+    far = spread(far_results)
+    near_results = apply_half(own_half, rows)
+    near_results, far = lax.optimization_barrier((near_results, far))
+    crossing = mix(mirror_target, mirror_shares, far).astype(jnp.bfloat16)
+    crossed = lax.ppermute(crossing, "fs", mirror)
+    near = spread(near_results)
+    mixed = mix(target, shares, near) + crossed.astype(jnp.float32)
     return (gate_serve, up_serve, down_serve, mixed.astype(jnp.bfloat16))
 
 

time: 304 us -> 292 us (0.961)
  waiting for transfers between devices: 221 us -> 189 us
  starting transfers between devices: 15.9 us -> 25.1 us
  Pallas kernels: 18.6 us -> 25.2 us
    all_to_all x1 -> x2, waiting for transfers between devices: 90.3 us -> 16.4 us  [spread(): lax.all_to_all(results.reshape(members, quarter, down_width), ('fs', 'tp'...]
    ppermute x0 -> x3, waiting for transfers between devices: none -> 44.5 us  [the longest x1 44.5 us: on_device(): crossed = lax.ppermute(crossing, 'fs', mirror)]
    all_to_all x1 -> x2, starting transfers between devices: 3.95 us -> 8.69 us  [spread(): lax.all_to_all(results.reshape(members, quarter, down_width), ('fs', 'tp'...]
    ppermute x0 -> x3, starting transfers between devices: none -> 4.44 us  [the longest x1 2.83 us: on_device(): mirror_target = lax.ppermute(target, 'fs', mirror)]
    pallas_call x1 -> x2, Pallas kernels: 11.3 us -> 15.2 us  [expert_hidden(): pl.pallas_call(hidden_kernel, grid_spec=pltpu.PrefetchScalarGridSpec(num_...]
    all_gather x1, waiting for transfers between devices: 21 us -> 17.9 us  [on_device(): gate_whole = lax.all_gather(gate_t, 'tp', axis=0, tiled=True)]
    pallas_call x1 -> x2, Pallas kernels: 7.29 us -> 10 us  [expert_out(): pl.pallas_call(down_kernel, grid=(sources // step_sources,), in_specs=[pl...]
    dot_general x1 -> x2, matrix products: 8.06 us -> 10.3 us  [mix(): jnp.dot(mixing.astype(jnp.bfloat16), values, preferred_element_type=jnp.f...]
  transfers between devices with their start and end apart: 6 -> 10, of which waited for: 5 -> 6; matrix products, arithmetic and copies ran while one was open for 6% -> 8% of each run, Pallas kernels for 4% -> 9%
where the time goes in v2:
time: 292 us; the launch traced here: 291 us
  waiting for transfers between devices  189 us (65%)
  Pallas kernels  25.2 us (9%)
  starting transfers between devices  25.1 us (9%)
  matrix products  16.8 us (6%)
  between operations  14 us (5%)
  other arithmetic  11.2 us (4%)
  local copies, waits for them, and re-layouts  9.21 us (3%)
    ppermute x1, waiting for transfers between devices, on_device(): crossed = lax.ppermute(crossing, 'fs', mirror)  44.5 us
    all_to_all x1, waiting for transfers between devices, on_device(): lax.all_to_all(outgoing, 'fs', split_axis=0, concat_axis=0, tiled=True)  40.3 us
    all_to_all x1, waiting for transfers between devices, on_device(): lax.all_to_all(packed, 'fs', split_axis=0, concat_axis=0, tiled=True)  39.5 us
    all_gather x1, waiting for transfers between devices, on_device(): up_whole = lax.all_gather(up_t, 'tp', axis=0, tiled=True)  30.7 us
    all_gather x1, waiting for transfers between devices, on_device(): gate_whole = lax.all_gather(gate_t, 'tp', axis=0, tiled=True)  17.9 us
    all_to_all x2, waiting for transfers between devices, spread(): lax.all_to_all(results.reshape(members, quarter, down_width), ('fs', 'tp'...  16.4 us
    pallas_call x2, Pallas kernels, expert_hidden(): pl.pallas_call(hidden_kernel, grid_spec=pltpu.PrefetchScalarGridSpec(num_...  15.2 us
    dot_general x2, matrix products, mix(): jnp.dot(mixing.astype(jnp.bfloat16), values, preferred_element_type=jnp.f...  10.3 us
  transfers between devices with their start and end apart: 10, of which 6 were waited for; matrix products, arithmetic and copies ran while one was open for 8% of the time, Pallas kernels for 9%

profile of v2, /device:TPU:0, one launch (start us, length us, event | category | flops | bytes accessed | tf_op | source)
XLA Modules:
  0.0 291.0 jit_solution(12237403756081384296)
XLA Ops:
  7.2 0.0 copy-start.3
  7.2 0.0 copy-start.2
  7.2 1.7 convert_element_type.56
  8.8 0.1 fusion.40
  8.9 0.1 copy-done.3
  9.0 0.5 copy-done.2
  9.5 1.0 fusion.31
  10.6 0.0 copy-start.4
  10.6 1.6 pad_maximum_fusion
  12.2 7.3 %all-to-all-start = ((bf16[8,576,256]{2,1,0:T(8,128)(2,1)}), bf16[8,576,256]{2,1,0:T(8,128)(2,1)S(1)}, u32[]{:S(2)}, u32[]{:S(2)}) async-start(bf16[8,576,256]{2,1,0:T(8,128)(2,1)} %pad_maximum_fusion), calls=%async_computation | async-start | bytes 4718592 | tf_op jit(solution)/shard_map/all_to_all | solution.py:96
  19.5 0.0 all-gather.5.cloned.1.call-start
  19.5 0.0 copy-done.4
  19.5 0.2 copy.27
  19.8 0.3 eq.108
  20.0 0.3 eq.104
  20.3 2.3 reduce-window.6
  22.6 0.3 slice_reduce_fusion
  22.9 0.2 reduce-window.9
  23.1 0.1 add_bitcast_fusion
  23.2 0.5 reduce_sum.30
  23.7 0.2 copy.29
  23.9 0.0 copy-start
  23.9 0.1 add_bitcast_fusion.1
  24.0 3.2 %fusion = f32[1024]{0:T(1024)S(1)} fusion(bf16[1024,2048]{1,0:T(8,128)(2,1)} %param.7), kind=kLoop, calls=%fused_computation.2 | loop fusion | flops 6290432 | bytes 4198400 | tf_op jit(solution)/shard_map/reduce_sum | solution.py:100
  27.2 0.1 copy-done
  27.3 6.5 %fusion.22 = bf16[1024,2048]{1,0:T(8,128)(2,1)} fusion(bf16[1024,2048]{1,0:T(8,128)(2,1)S(1)} %copy-done, f32[1024]{0:T(1024)S(1)} %add_rsqrt_fusion, s32[1024]{0:T(1024)S(1)} %bitcast.81, s32[1024]{0:T(1024)S(1)} %bitcast.79, s32[1024]{0:T(1024)S(1)} %add_bitcast_fusion.1), kind=kOutput, calls=%fused_computation.25 | convolution fusion | flops 4306501632 | bytes 8404992 | tf_op jit(solution)/shard_map/dot_general | solution.py:114
  33.8 39.5 %all-to-all-done = bf16[8,576,256]{2,1,0:T(8,128)(2,1)S(1)} async-done(((bf16[8,576,256]{2,1,0:T(8,128)(2,1)}), bf16[8,576,256]{2,1,0:T(8,128)(2,1)S(1)}, u32[]{:S(2)}, u32[]{:S(2)}) %all-to-all-start) | async-done | bytes 2359328 | tf_op jit(solution)/shard_map/all_to_all | solution.py:96
  73.3 0.1 slice_bitcast_fusion
  73.5 1.0 copy.33
  74.4 0.0 all-gather.5.cloned.1.call-update
  74.5 0.0 all-gather.7.cloned.1.call-start
  74.5 1.0 copy.34
  75.5 0.0 all-gather.7.cloned.1.call-update
  75.5 0.0 copy-start.5
  75.5 4.6 %all-to-all-start.1 = ((bf16[8,128,2048]{2,1,0:T(8,128)(2,1)}), bf16[8,128,2048]{2,1,0:T(8,128)(2,1)}, u32[]{:S(2)}, u32[]{:S(2)}) async-start(bf16[8,128,2048]{2,1,0:T(8,128)(2,1)} %bitcast.69), calls=%async_computation.1 | async-start | bytes 8388608 | tf_op jit(solution)/shard_map/all_to_all | solution.py:119
  80.1 0.0 all-gather.9.cloned.1.call-start
  80.1 0.1 fusion.39
  80.2 0.9 pad_maximum_fusion.1
  81.1 0.0 all-gather.9.cloned.1.call-update
  81.2 2.8 collective-permute-start
  84.0 0.0 copy-done.5
  84.0 0.2 collective-permute-start.1
  84.3 17.9 %all-gather.5.cloned.1.call-done.gate_ref = bf16[768,2048]{1,0:T(8,128)(2,1)} async-done(((bf16[192,2048]{1,0:T(8,128)(2,1)}), bf16[768,2048]{1,0:T(8,128)(2,1)}) %all-gather.5.cloned.1.call-update) | async-done | bytes 3145744 | tf_op jit(solution)/shard_map/all_gather | solution.py:135
  102.2 30.7 %all-gather.7.cloned.1.call-done.up_ref = bf16[768,2048]{1,0:T(8,128)(2,1)} async-done(((bf16[192,2048]{1,0:T(8,128)(2,1)}), bf16[768,2048]{1,0:T(8,128)(2,1)}) %all-gather.7.cloned.1.call-update) | async-done | bytes 3145744 | tf_op jit(solution)/shard_map/all_gather | solution.py:136
  132.8 40.3 %all-to-all-done.1 = bf16[8,128,2048]{2,1,0:T(8,128)(2,1)} async-done(((bf16[8,128,2048]{2,1,0:T(8,128)(2,1)}), bf16[8,128,2048]{2,1,0:T(8,128)(2,1)}, u32[]{:S(2)}, u32[]{:S(2)}) %all-to-all-start.1) | async-done | bytes 4194336 | tf_op jit(solution)/shard_map/all_to_all | solution.py:119
  173.2 7.6 %expert_hidden.2.hidden_ref = bf16[512,768]{1,0:T(8,128)(2,1)} custom-call(s32[1]{0:T(128)} %bitcast.20.first_ref, bf16[1024,2048]{1,0:T(8,128)(2,1)} %bitcast.21.rows_ref, bf16[768,2048]{1,0:T(8,128)(2,1)} %all-gather.5.cloned.1.call-done.gate_ref, bf16[768,2048]{1,0:T(8,128)(2,1)} %all-gather.7.cloned.1.call-done.up_ref), custom_call_target="tpu_custom_call" | custom-call | flops 3221225472 | bytes 9175040 | tf_op jit(solution)/shard_map/expert_hidden/pallas_call | solution.py:31
  180.8 0.0 all-gather.9.cloned.1.call-done
  180.8 5.0 %expert_out.2 = bf16[4,4,128,512]{3,2,1,0:T(8,128)(2,1)} custom-call(bf16[512,768]{1,0:T(8,128)(2,1)} %expert_hidden.2.hidden_ref, bf16[4,768,512]{2,1,0:T(8,128)(2,1)} %bitcast.64), custom_call_target="tpu_custom_call" | custom-call | flops 1610612736 | bytes 6029312 | tf_op jit(solution)/shard_map/expert_out/pallas_call | solution.py:57
  185.8 0.0 collective-permute-done
  185.8 0.0 collective-permute-done.1
  185.8 3.8 %all-to-all-start.2 = ((bf16[16,128,512]{2,1,0:T(8,128)(2,1)}), bf16[16,128,512]{2,1,0:T(8,128)(2,1)S(1)}, u32[]{:S(2)}, u32[]{:S(2)}) async-start(bf16[16,128,512]{2,1,0:T(8,128)(2,1)} %bitcast.68), calls=%async_computation.2 | async-start | bytes 4194304 | tf_op jit(solution)/shard_map/all_to_all | solution.py:161
  189.6 7.6 %expert_hidden.3.hidden_ref = bf16[512,768]{1,0:T(8,128)(2,1)} custom-call(s32[1]{0:T(128)} %bitcast.19.first_ref, bf16[1024,2048]{1,0:T(8,128)(2,1)} %bitcast.21.rows_ref, bf16[768,2048]{1,0:T(8,128)(2,1)} %all-gather.5.cloned.1.call-done.gate_ref, bf16[768,2048]{1,0:T(8,128)(2,1)} %all-gather.7.cloned.1.call-done.up_ref), custom_call_target="tpu_custom_call" | custom-call | flops 3221225472 | bytes 9175040 | tf_op jit(solution)/shard_map/expert_hidden/pallas_call | solution.py:31
  197.2 5.0 %expert_out.3 = bf16[4,4,128,512]{3,2,1,0:T(8,128)(2,1)} custom-call(bf16[512,768]{1,0:T(8,128)(2,1)} %expert_hidden.3.hidden_ref, bf16[4,768,512]{2,1,0:T(8,128)(2,1)} %bitcast.65), custom_call_target="tpu_custom_call" | custom-call | flops 1610612736 | bytes 6029312 | tf_op jit(solution)/shard_map/expert_out/pallas_call | solution.py:57
  202.2 16.4 %all-to-all-done.2 = bf16[16,128,512]{2,1,0:T(8,128)(2,1)S(1)} async-done(((bf16[16,128,512]{2,1,0:T(8,128)(2,1)}), bf16[16,128,512]{2,1,0:T(8,128)(2,1)S(1)}, u32[]{:S(2)}, u32[]{:S(2)}) %all-to-all-start.2) | async-done | bytes 2097184 | tf_op jit(solution)/shard_map/all_to_all | solution.py:161
  218.6 1.3 copy-done.1
  220.0 4.9 %all-to-all-start.3 = ((bf16[16,128,512]{2,1,0:T(8,128)(2,1)}), bf16[16,128,512]{2,1,0:T(8,128)(2,1)S(1)}, u32[]{:S(2)}, u32[]{:S(2)}) async-start(bf16[16,128,512]{2,1,0:T(8,128)(2,1)} %bitcast.67), calls=%async_computation.3 | async-start | bytes 4194304 | tf_op jit(solution)/shard_map/all_to_all | solution.py:161
  224.9 5.3 %fusion.30 = bf16[1024,512]{1,0:T(8,128)(2,1)} fusion(bf16[2048,512]{1,0:T(8,128)(2,1)} %bitcast.75, f32[1024]{0:T(1024)S(1)} %bitcast.88, f32[1024]{0:T(1024)S(1)} %bitcast.87, s32[2048]{0:T(1024)S(1)} %iota_add_fusion, s32[1024]{0:T(1024)S(1)} %bitcast.86, s32[1024]{0:T(1024)S(1)} %bitcast.85), kind=kOutput, calls=%fused_computation.33 | convolution fusion | flops 2156396544 | bytes 3170304 | tf_op jit(solution)/shard_map/dot_general | solution.py:178
  230.3 1.4 collective-permute-start.2
  231.7 1.2 dynamic-slice_bitcast_fusion
  232.9 0.6 copy.32
  233.5 1.5 reshape.110
  234.9 44.5 %collective-permute-done.2 = bf16[1024,512]{1,0:T(8,128)(2,1)} collective-permute-done((bf16[1024,512]{1,0:T(8,128)(2,1)}, bf16[1024,512]{1,0:T(8,128)(2,1)}, u32[]{:S(2)}, u32[]{:S(2)}) %collective-permute-start.2) | collective-permute-done | bytes 1048608 | tf_op jit(solution)/shard_map/ppermute | solution.py:191
  279.5 0.0 all-to-all-done.3
  279.5 5.0 %add_convert_fusion = bf16[1024,512]{1,0:T(8,128)(2,1)} fusion(bf16[1024,512]{1,0:T(8,128)(2,1)} %collective-permute-done.2, bf16[2048,512]{1,0:T(8,128)(2,1)S(1)} %bitcast.74, f32[1024]{0:T(1024)S(1)} %bitcast.84, f32[1024]{0:T(1024)S(1)} %bitcast.83, s32[2048]{0:T(1024)S(1)} %iota_add_fusion, s32[1024]{0:T(1024)S(1)} %bitcast.80, s32[1024]{0:T(1024)S(1)} %bitcast.82), kind=kOutput, calls=%fused_computation.27 | convolution fusion | flops 2157445120 | bytes 4218880 | tf_op jit(solution)/shard_map/dot_general | solution.py:178
  (13 shorter events, 0.1 us)
Async XLA Ops:
  7.2 1.9 copy-start.3
  7.2 2.3 copy-start.2
  10.6 9.0 %copy-start.4 = (s32[1024,2]{0,1:T(2,128)S(1)}, s32[1024,2]{0,1:T(2,128)}, u32[]{:S(2)}) copy-start(s32[1024,2]{0,1:T(2,128)} %param.12) | copy-start | bytes 24580
  12.2 61.2 %all-to-all-start = ((bf16[8,576,256]{2,1,0:T(8,128)(2,1)}), bf16[8,576,256]{2,1,0:T(8,128)(2,1)S(1)}, u32[]{:S(2)}, u32[]{:S(2)}) async-start(bf16[8,576,256]{2,1,0:T(8,128)(2,1)} %pad_maximum_fusion), calls=%async_computation | async-start | bytes 4718592 | tf_op jit(solution)/shard_map/all_to_all | solution.py:96
  19.5 82.7 %all-gather.5.cloned.1.call-start = ((), (), s32[]{:S(2)}) async-start(), calls=%async_computation.4 | async-start | bytes 3932160 | tf_op jit(solution)/shard_map/all_gather | solution.py:135
  23.9 3.5 %copy-start = (bf16[1024,2048]{1,0:T(8,128)(2,1)S(1)}, bf16[1024,2048]{1,0:T(8,128)(2,1)}, u32[]{:S(2)}) copy-start(bf16[1024,2048]{1,0:T(8,128)(2,1)} %param.7) | copy-start | bytes 12582916
  74.5 58.4 %all-gather.7.cloned.1.call-start = ((), (), s32[]{:S(2)}) async-start(), calls=%async_computation.5 | async-start | bytes 3932160 | tf_op jit(solution)/shard_map/all_gather | solution.py:136
  75.5 8.5 %copy-start.5 = (f32[1024,2]{0,1:T(2,128)S(1)}, f32[1024,2]{0,1:T(2,128)}, u32[]{:S(2)}) copy-start(f32[1024,2]{0,1:T(2,128)} %param.13) | copy-start | bytes 24580
  75.5 97.7 %all-to-all-start.1 = ((bf16[8,128,2048]{2,1,0:T(8,128)(2,1)}), bf16[8,128,2048]{2,1,0:T(8,128)(2,1)}, u32[]{:S(2)}, u32[]{:S(2)}) async-start(bf16[8,128,2048]{2,1,0:T(8,128)(2,1)} %bitcast.69), calls=%async_computation.1 | async-start | bytes 8388608 | tf_op jit(solution)/shard_map/all_to_all | solution.py:119
  80.1 100.7 %all-gather.9.cloned.1.call-start = ((), (), s32[]{:S(2)}) async-start(), calls=%async_computation.6 | async-start | bytes 3932160 | tf_op jit(solution)/shard_map/all_gather | solution.py:137
  81.2 104.6 %collective-permute-start = (s32[1024,2]{0,1:T(2,128)S(1)}, s32[1024,2]{0,1:T(2,128)S(1)}, u32[]{:S(2)}, u32[]{:S(2)}) collective-permute-start(s32[1024,2]{0,1:T(2,128)S(1)} %multiply_add_fusion), channel_id=1, source_target_pairs={{0,16},{4,20},{8,24},{12,28},{16,0},{20,4},{24,8},{28,12},{1,17},{... | collective-permute-start | bytes 24584 | tf_op jit(solution)/shard_map/ppermute | solution.py:181
  84.0 101.8 %collective-permute-start.1 = (f32[1024,2]{0,1:T(2,128)S(1)}, f32[1024,2]{0,1:T(2,128)S(1)}, u32[]{:S(2)}, u32[]{:S(2)}) collective-permute-start(f32[1024,2]{0,1:T(2,128)S(1)} %broadcast_divide_fusion), channel_id=1, source_target_pairs={{0,16},{4,20},{8,24},{12,28},{16,0},{20,4},{24,8},{28,12},{1,17},{... | collective-permute-start | bytes 24584 | tf_op jit(solution)/shard_map/ppermute | solution.py:182
  185.8 32.8 %all-to-all-start.2 = ((bf16[16,128,512]{2,1,0:T(8,128)(2,1)}), bf16[16,128,512]{2,1,0:T(8,128)(2,1)S(1)}, u32[]{:S(2)}, u32[]{:S(2)}) async-start(bf16[16,128,512]{2,1,0:T(8,128)(2,1)} %bitcast.68), calls=%async_computation.2 | async-start | bytes 4194304 | tf_op jit(solution)/shard_map/all_to_all | solution.py:161
  218.6 1.3 copy-start.1
  220.0 59.5 %all-to-all-start.3 = ((bf16[16,128,512]{2,1,0:T(8,128)(2,1)}), bf16[16,128,512]{2,1,0:T(8,128)(2,1)S(1)}, u32[]{:S(2)}, u32[]{:S(2)}) async-start(bf16[16,128,512]{2,1,0:T(8,128)(2,1)} %bitcast.67), calls=%async_computation.3 | async-start | bytes 4194304 | tf_op jit(solution)/shard_map/all_to_all | solution.py:161
  230.3 49.2 %collective-permute-start.2 = (bf16[1024,512]{1,0:T(8,128)(2,1)}, bf16[1024,512]{1,0:T(8,128)(2,1)}, u32[]{:S(2)}, u32[]{:S(2)}) collective-permute-start(bf16[1024,512]{1,0:T(8,128)(2,1)} %fusion.30), channel_id=1, source_target_pairs={{0,16},{4,20},{8,24},{12,28},{16,0},{20,4},{24,8},{28,12},{1,17},{... | collective-permute-start | bytes 3145736 | tf_op jit(solution)/shard_map/ppermute | solution.py:191
Sparse Core Ops, SparseCore 0:
  74.6 27.5 all-gather.4
  104.3 28.4 all-gather.6
  135.0 28.4 all-gather.8
